TPU v7x, 512 devices: a whole 4x8x8 slice. The times are simulated.
512 devices in a mesh: sp: 64 (over z, y), fs: 4 (over x), tp: 2 (over core).
Axes of the slice: x: 4, y: 8, z: 8, core: 2. Of those that a mesh axis runs over, the one named last changes fastest.
Arguments:
- tokens: bfloat16 [4, 16384, 1024], P('fs', 'sp', 'tp'), may hold values from -6 to 6
- w_inner: bfloat16 [1024, 2048], P('sp', 'tp'), may hold values from -0.1875 to 0.1875
- w_gate: bfloat16 [1024, 2048], P('sp', 'tp'), may hold values from -0.1875 to 0.1875
- w_write: bfloat16 [1024, 512], P('sp', 'tp'), may hold values from -0.1875 to 0.1875
- w_read: bfloat16 [1024, 512], P('sp', 'tp'), may hold values from -0.1875 to 0.1875
- w_pool_in: bfloat16 [1024, 1024], P('sp', 'tp'), may hold values from -0.1875 to 0.1875
- w_step: bfloat16 [1024, 2, 32], replicated, may hold values from -0.1875 to 0.1875
- conv_inner: bfloat16 [5, 2048], replicated, may hold values from -2.5 to 2.5
- conv_cross: bfloat16 [5, 2, 512], replicated, may hold values from -2.5 to 2.5
- rate_log: float32 [2, 32], replicated, may hold values from -20 to -3
- decay_extra: float32 [4, 16384, 2, 32], P('fs', 'sp', None, 'tp'), may hold values from -1 to 0
- norm_gain: float32 [2048], replicated, may hold values from 0.1 to 1.9
- pool_mix: bfloat16 [4, 256, 256], replicated, may hold values from -0.375 to 0.375
- pool_gain: float32 [1024], replicated, may hold values from 0.1 to 1.9
- w_out_inner: bfloat16 [2048, 1024], P('tp', 'fs'), may hold values from -0.109375 to 0.109375
- w_out_pool: bfloat16 [1024, 1024], P('tp', 'fs'), may hold values from -0.109375 to 0.109375
Outputs:
- layer_out: bfloat16 [4, 16384, 1024], P('fs', ('sp', 'tp'))
All inputs are finite; a program needn't handle non-finite values.
Results may differ from a plain program's by a relative error of at most 0.0075.
Values may be sent and summed in bfloat16 or wider, within the bound.
A program may use at most 128 MiB of HBM per device.

v0:
```python
import jax
import jax.numpy as jnp
from jax import lax
from jax.sharding import Mesh
from jax.sharding import PartitionSpec as P

HEAD_DIM = 64
STATE = 128
POOL_DIM = 256
POOL_GROUPS = 4
CONV = 5
BLOCK = 128
GRID_W = 32
SP = ("sp_0", "sp_1")
SP_TP = ("sp_0", "sp_1", "tp")
EPSILON = 1e-05


def with_halo(block, sides, width):
    for axis, dim in sides:
        count = lax.axis_size(axis)
        forward = [(i, i + 1) for i in range(count - 1)]
        backward = [(target, source) for source, target in forward]
        low = lax.ppermute(
            lax.slice_in_dim(block, block.shape[dim] - width, None, axis=dim), axis, forward
        )
        high = lax.ppermute(lax.slice_in_dim(block, 0, width, axis=dim), axis, backward)
        block = jnp.concatenate([low, block, high], axis=dim)
    return block


def sent_together(arrays, axis, dim, along):
    ends, at = ([], 0)
    for a in arrays[:-1]:
        at += a.shape[along]
        ends.append(at)
    both = jnp.concatenate(arrays, axis=along)
    return tuple(jnp.split(lax.all_gather(both, axis, axis=dim, tiled=True), ends, axis=along))


def sent_to_all(value, axis):
    devices = lax.axis_size(axis)
    return lax.all_to_all(
        jnp.broadcast_to(value[None], (devices, *value.shape)), axis, 0, 0, tiled=True
    )


def in_order(pieces, dim):
    pieces = jnp.moveaxis(pieces, 0, dim)
    lengths = pieces.shape
    return pieces.reshape(*lengths[:dim], lengths[dim] * lengths[dim + 1], *lengths[dim + 2 :])


def gather_directly(value, axis, dim):
    pieces = sent_to_all(value, axis)
    return in_order(pieces, dim)


def nothing_yet(value, identity):
    return jax.tree.map(
        lambda part, zero: jnp.zeros_like(part) + jnp.asarray(zero, part.dtype), value, identity
    )


def prefix_by_axis(value, axes, combine, identity, reverse):
    before = start = nothing_yet(value, identity)
    subtotal = value
    for axis in reversed(axes):
        devices, mine = (lax.axis_size(axis), lax.axis_index(axis))
        pieces = jax.tree.map(
            lambda part, kind: lax.all_gather(part.astype(kind), axis),
            subtotal,
            jax.tree.map(lambda a: jnp.bfloat16 if a.dtype == jnp.float32 else a.dtype, value),
        )
        inside, subtotal = (start, start)
        for k in reversed(range(devices)) if reverse else range(devices):
            passed = k > mine if reverse else k < mine
            subtotal = combine(
                subtotal, jax.tree.map(lambda part, own: part[k].astype(own.dtype), pieces, value)
            )
            inside = jax.tree.map(lambda new, old: jnp.where(passed, new, old), subtotal, inside)
        before = combine(inside, before)
    return before


def cut_along(value, dim, devices):
    before, after = (value.shape[:dim], value.shape[dim + 1 :])
    return jnp.moveaxis(value.reshape(*before, devices, -1, *after), dim, 0)


def sum_at_owner(value, axis, dim):
    pieces = cut_along(value, dim, lax.axis_size(axis))
    arrived = lax.all_to_all(pieces, axis, split_axis=0, concat_axis=0, tiled=True)
    return arrived.astype(jnp.float32).sum(axis=0)


def merge_states(earlier, later):
    return (earlier[0] + later[0], earlier[1] * jnp.exp(later[0])[:, None, None] + later[1])


def local_summary(values, decays, writer_rows, read_rows, per_group):
    tokens_here, heads_here, head_width = values.shape
    groups_here = writer_rows.shape[1]
    blocks = tokens_here // BLOCK
    block_values = values.reshape(blocks, BLOCK, groups_here, per_group, head_width)
    cumulative = jnp.cumsum(
        jnp.transpose(decays.reshape(blocks, BLOCK, heads_here), (0, 2, 1)), axis=2
    )
    cumulative = cumulative.reshape(blocks, groups_here, per_group, BLOCK)
    writes_group = writer_rows.reshape(blocks, BLOCK, groups_here, STATE)
    reads_group = read_rows.reshape(blocks, BLOCK, groups_here, STATE)
    lower_mask = jnp.tril(jnp.ones((BLOCK, BLOCK), dtype=bool))
    segment_log = cumulative[..., :, None] - cumulative[..., None, :]
    weights = jnp.exp(jnp.where(lower_mask, segment_log, -jnp.inf))
    scores = jnp.einsum("bign,bjgn->bgij", reads_group, writes_group)
    inside = jnp.einsum("bgrij,bjgrp->bigrp", scores[:, :, None] * weights, block_values)
    tail_decay = jnp.exp(cumulative[..., -1:] - cumulative)
    block_states = jnp.einsum("bjgn,bgrj,bjgrp->bgrpn", writes_group, tail_decay, block_values)
    block_decay = cumulative[..., -1]
    block_ends = jnp.cumsum(block_decay, axis=0)
    starts = block_ends - block_decay
    order = jnp.arange(blocks, dtype=jnp.int32)
    earlier_mask = (order[:, None] > order[None, :])[:, :, None, None]
    link_decay = jnp.exp(jnp.where(earlier_mask, starts[:, None] - block_ends[None], -jnp.inf))
    entering = jnp.einsum("bcgr,cgrpn->bgrpn", link_decay, block_states)
    device_decay = block_ends[-1]
    summary = jnp.einsum("cgr,cgrpn->grpn", jnp.exp(device_decay[None] - block_ends), block_states)
    parts = (inside, cumulative, starts, entering, reads_group)
    return (
        parts,
        (device_decay.reshape(heads_here), summary.reshape(heads_here, head_width, STATE)),
    )


def finish(parts, incoming):
    inside, cumulative, starts, entering, reads_group = parts
    blocks, groups_here, per_group, block_len = cumulative.shape
    arriving = incoming[1].reshape(
        groups_here, per_group, incoming[1].shape[1], incoming[1].shape[2]
    )
    entering = entering + jnp.exp(starts)[..., None, None] * arriving[None]
    carried = jnp.einsum("bign,bgrpn->bigrp", reads_group, entering)
    carried = carried * jnp.transpose(jnp.exp(cumulative), (0, 3, 1, 2))[..., None]
    outcome = inside + carried
    return outcome.reshape(blocks * block_len, groups_here * per_group, outcome.shape[4])


def pool_local(pool_in, pool_mix, pool_gain, tp_rank, position, devices):
    reach_rows = 2 ** (POOL_GROUPS - 1)
    tokens_here = pool_in.shape[0]
    channels = pool_in.shape[1]
    groups_here = channels // POOL_DIM
    grid_rows = tokens_here // GRID_W
    all_rows = grid_rows * devices
    framed = with_halo(pool_in, ((SP, 0),), reach_rows * GRID_W)
    framed = framed.astype(jnp.float32).reshape(
        grid_rows + 2 * reach_rows, GRID_W, groups_here, POOL_DIM
    )
    row_running = jnp.cumsum(jnp.pad(framed, ((1, 0), (0, 0), (0, 0), (0, 0))), axis=0)
    row_index = position * grid_rows + jnp.arange(grid_rows, dtype=jnp.int32)
    col_index = jnp.arange(GRID_W, dtype=jnp.int32)
    mix_local = lax.dynamic_slice_in_dim(pool_mix, tp_rank * groups_here, groups_here, 0)
    gain_local = lax.dynamic_slice_in_dim(pool_gain, tp_rank * channels, channels, 0)
    results = []
    for slot_index in range(groups_here):
        group_index = tp_rank * groups_here + slot_index
        window = jnp.left_shift(jnp.int32(2), group_index)
        half_window = window // 2
        row_band = row_running[:, :, slot_index]
        box_sum = lax.dynamic_slice_in_dim(
            row_band, reach_rows - half_window + window, grid_rows, 0
        ) - lax.dynamic_slice_in_dim(row_band, reach_rows - half_window, grid_rows, 0)
        col_running = jnp.cumsum(
            jnp.pad(box_sum, ((0, 0), (reach_rows + 1, reach_rows), (0, 0))), axis=1
        )
        box_sum = lax.dynamic_slice_in_dim(
            col_running, reach_rows - half_window + window, GRID_W, 1
        ) - lax.dynamic_slice_in_dim(col_running, reach_rows - half_window, GRID_W, 1)
        row_counts = (
            jnp.clip(row_index - half_window + window, 0, all_rows)
            - jnp.clip(row_index - half_window, 0, all_rows)
        ).astype(jnp.float32)
        col_counts = (
            jnp.clip(col_index - half_window + window, 0, GRID_W)
            - jnp.clip(col_index - half_window, 0, GRID_W)
        ).astype(jnp.float32)
        average = box_sum / (row_counts[:, None, None] * col_counts[None, :, None])
        own_values = framed[reach_rows : reach_rows + grid_rows, :, slot_index]
        offsets = (average - own_values).astype(jnp.bfloat16).reshape(tokens_here, POOL_DIM)
        mixed_rows = jnp.dot(offsets, mix_local[slot_index], preferred_element_type=jnp.float32)
        gain_part = gain_local[slot_index * POOL_DIM : (slot_index + 1) * POOL_DIM]
        results.append((mixed_rows * gain_part).astype(jnp.bfloat16))
    return jnp.concatenate(results, axis=1)


def body(
    tokens,
    w_inner,
    w_gate,
    w_write,
    w_read,
    w_pool_in,
    w_step,
    conv_inner,
    conv_cross,
    rate_log,
    decay_extra,
    norm_gain,
    pool_mix,
    pool_gain,
    w_out_inner,
    w_out_pool,
):
    tp_rank = lax.axis_index("tp")
    out_weights = sent_together((w_out_inner, w_out_pool), "fs", 1, 0)
    whole_rows = gather_directly(tokens[0], "tp", 1)
    tokens_here = whole_rows.shape[0]
    inner_here = w_inner.shape[1]
    cross_here = w_write.shape[1]
    heads_here = inner_here // HEAD_DIM
    groups_here = cross_here // STATE
    per_group = heads_here // groups_here
    stacked = jnp.concatenate([w_inner, w_write, w_read, w_gate, w_pool_in], axis=1)
    projected = jnp.dot(
        whole_rows,
        lax.all_gather(stacked, SP, axis=0, tiled=True),
        preferred_element_type=jnp.float32,
    )
    projected = projected.astype(jnp.bfloat16)
    stream_cols = inner_here + 2 * cross_here
    streams = projected[:, :stream_cols]
    gate_in = projected[:, stream_cols : stream_cols + inner_here]
    pool_in = projected[:, stream_cols + inner_here :]
    rim_width = CONV // 2
    framed = with_halo(streams, ((SP, 0),), rim_width).astype(jnp.float32)
    conv_taps = jnp.concatenate(
        [
            lax.dynamic_slice_in_dim(conv_inner, tp_rank * inner_here, inner_here, 1),
            lax.dynamic_slice_in_dim(conv_cross[:, 0], tp_rank * cross_here, cross_here, 1),
            lax.dynamic_slice_in_dim(conv_cross[:, 1], tp_rank * cross_here, cross_here, 1),
        ],
        axis=1,
    ).astype(jnp.float32)
    running = jnp.zeros((tokens_here, stream_cols), jnp.float32)
    for offset in range(CONV):
        running = running + framed[offset : offset + tokens_here] * conv_taps[offset]
    activated = jax.nn.silu(running)
    values = activated[:, :inner_here].reshape(tokens_here, heads_here, HEAD_DIM)
    writer_rows = activated[:, inner_here : inner_here + cross_here].reshape(
        tokens_here, groups_here, STATE
    )
    read_rows = activated[:, inner_here + cross_here :].reshape(tokens_here, groups_here, STATE)
    step_weights = lax.dynamic_slice_in_dim(w_step, tp_rank * heads_here, heads_here, 2)
    raw_step = jnp.dot(
        whole_rows,
        step_weights.reshape(step_weights.shape[0], 2 * heads_here),
        preferred_element_type=jnp.float32,
    ).reshape(tokens_here, 2, heads_here)
    step_size = jax.nn.softplus(raw_step)
    decay_rates = jnp.exp(lax.dynamic_slice_in_dim(rate_log, tp_rank * heads_here, heads_here, 1))
    log_decay = -step_size * decay_rates[None] + decay_extra[0]
    ahead_parts, ahead_summary = local_summary(
        values * step_size[:, 0, :, None], log_decay[:, 0], writer_rows, read_rows, per_group
    )
    behind_parts, behind_summary = local_summary(
        (values * step_size[:, 1, :, None])[::-1],
        log_decay[::-1, 1],
        writer_rows[::-1],
        read_rows[::-1],
        per_group,
    )
    blank_state = (jnp.zeros_like(ahead_summary[0]), jnp.zeros_like(ahead_summary[1]))
    ahead_in = prefix_by_axis(ahead_summary, SP, merge_states, blank_state, False)
    behind_in = prefix_by_axis(behind_summary, SP, merge_states, blank_state, True)
    pooled = pool_local(
        pool_in, pool_mix, pool_gain, tp_rank, lax.axis_index(SP), lax.axis_size(SP)
    )
    mixed_sum = finish(ahead_parts, ahead_in) + finish(behind_parts, behind_in)[::-1]
    gated_out = mixed_sum * jax.nn.silu(gate_in.astype(jnp.float32)).reshape(
        tokens_here, heads_here, HEAD_DIM
    )
    rms_scale = lax.rsqrt(jnp.mean(gated_out * gated_out, axis=2, keepdims=True) + EPSILON)
    gain_local = lax.dynamic_slice_in_dim(norm_gain, tp_rank * inner_here, inner_here, 0).reshape(
        heads_here, HEAD_DIM
    )
    mixer_out = (
        (gated_out * rms_scale * gain_local).reshape(tokens_here, inner_here).astype(jnp.bfloat16)
    )
    inner_weights, pool_weights = out_weights
    summed = sum_at_owner(
        (
            jnp.dot(mixer_out, inner_weights, preferred_element_type=jnp.float32)
            + jnp.dot(pooled, pool_weights, preferred_element_type=jnp.float32)
        ).astype(jnp.bfloat16),
        "tp",
        0,
    )
    return summed.astype(jnp.bfloat16)[None]


def solution(mesh):
    finer = Mesh(
        mesh.devices.reshape(8, 8, mesh.shape["fs"], mesh.shape["tp"]), ("sp_0", "sp_1", "fs", "tp")
    )
    in_specs = (
        P("fs", SP, "tp"),
        P(SP, "tp"),
        P(SP, "tp"),
        P(SP, "tp"),
        P(SP, "tp"),
        P(SP, "tp"),
        P(),
        P(),
        P(),
        P(),
        P("fs", SP, None, "tp"),
        P(),
        P(),
        P(),
        P("tp", "fs"),
        P("tp", "fs"),
    )
    out_specs = P("fs", SP_TP, None)
    return jax.shard_map(body, mesh=finer, in_specs=in_specs, out_specs=out_specs, check_vma=False)
```

profile of v0, /device:TPU:1, one launch (start us, length us, event | category | flops | bytes accessed | tf_op | source)
XLA Modules:
  0.0 369.2 jit_solution(7352323665303950627)
XLA Ops:
  12.9 10.3 %all-to-all-start = ((bf16[2,256,512]{1,2,0:T(8,128)(2,1)}), bf16[2,256,512]{1,2,0:T(8,128)(2,1)S(1)}, u32[]{:S(2)}, u32[]{:S(2)}) async-start(bf16[2,256,512]{1,2,0:T(8,128)(2,1)} %broadcast_in_dim.44), calls=%async_computation | async-start | bytes 1048576 | tf_op jit(solution)/shard_map/all_to_all | solution.py:43
  27.1 78.8 %all-gather.11.cloned.1.call-done = bf16[1024,3072]{1,0:T(8,128)(2,1)} async-done(((bf16[16,3072]{1,0:T(8,128)(2,1)}), bf16[1024,3072]{1,0:T(8,128)(2,1)}) %all-gather.11.cloned.1.call-update) | async-done | bytes 6291472 | tf_op jit(solution)/shard_map/all_gather | solution.py:226
  105.9 4.6 %fusion = bf16[256,3072]{1,0:T(8,128)(2,1)S(1)} fusion(bf16[1024,3072]{1,0:T(8,128)(2,1)} %all-gather.11.cloned.1.call-done, bf16[256,1024]{0,1:T(8,128)(2,1)S(1)} %bitcast.451), kind=kOutput, calls=%fused_computation.1 | convolution fusion | flops 1611399168 | bytes 8388608 | tf_op jit(solution)/shard_map/dot_general | solution.py:224
  111.9 4.0 %collective-permute-start = (bf16[2,1536]{1,0:T(2,128)(2,1)S(1)}, bf16[2,1536]{1,0:T(2,128)(2,1)S(1)}, u32[]{:S(2)}, u32[]{:S(2)}) collective-permute-start(bf16[2,1536]{1,0:T(2,128)(2,1)S(1)} %get-tuple-element.94), channel_id=1, source_target_pairs={{0,8},{8,16},{16,24},{24,32},{32,40},{40,48},{48,56},{56,64},{64,7... | collective-permute-start | bytes 18440 | tf_op jit(solution)/shard_map/ppermute | solution.py:24
  119.1 1.5 broadcast_multiply_fusion.2
  124.8 1.4 rev.15
  126.1 1.7 reshape.1089
  130.5 14.0 %all-gather = bf16[8,1,16]{2,1,0:T(2,128)(2,1)S(1)} all-gather(bf16[1,1,16]{2,1,0:T(2,128)(2,1)S(1)} %reshape.1178), channel_id=1, replica_groups=mesh['sp_0'=8,'sp_1'=8,'fs'=4,'tp'=2] {'sp_1'}, dimensions={0}, use_global_device_ids=true | all-gather | bytes 288 | tf_op jit(solution)/shard_map/all_gather | solution.py:71
  144.6 19.8 %all-gather.13.cloned.1.call-done = bf16[8,16,64,128]{3,2,1,0:T(8,128)(2,1)} async-done(((bf16[1,16,64,128]{3,2,1,0:T(8,128)(2,1)}), bf16[8,16,64,128]{3,2,1,0:T(8,128)(2,1)}) %all-gather.13.cloned.1.call-update) | async-done | bytes 2097168 | tf_op jit(solution)/shard_map/all_gather | solution.py:71
  164.5 2.7 add_convert_fusion.1
  167.4 11.4 %all-gather.2 = bf16[8,1,16]{2,1,0:T(2,128)(2,1)S(1)} all-gather(bf16[1,1,16]{2,1,0:T(2,128)(2,1)S(1)} %reshape.1182), channel_id=1, replica_groups=mesh['sp_0'=8,'sp_1'=8,'fs'=4,'tp'=2] {'sp_1'}, dimensions={0}, use_global_device_ids=true | all-gather | bytes 288 | tf_op jit(solution)/shard_map/all_gather | solution.py:71
  178.9 29.9 %all-gather.17.cloned.1.call-done = bf16[8,16,64,128]{3,2,1,0:T(8,128)(2,1)} async-done(((bf16[1,16,64,128]{3,2,1,0:T(8,128)(2,1)}), bf16[8,16,64,128]{3,2,1,0:T(8,128)(2,1)}) %all-gather.17.cloned.1.call-update) | async-done | bytes 2097168 | tf_op jit(solution)/shard_map/all_gather | solution.py:71
  208.8 2.7 add_convert_fusion
  221.8 13.7 %all-gather.3 = bf16[8,1,16]{2,1,0:T(2,128)(2,1)S(1)} all-gather(bf16[1,1,16]{2,1,0:T(2,128)(2,1)S(1)} %get-tuple-element.46), channel_id=1, replica_groups=mesh['sp_0'=8,'sp_1'=8,'fs'=4,'tp'=2] {'sp_0'}, dimensions={0}, use_global_device_ids=true | all-gather | bytes 288 | tf_op jit(solution)/shard_map/all_gather | solution.py:71
  235.5 12.3 %all-gather.1 = bf16[8,1,16]{2,1,0:T(2,128)(2,1)S(1)} all-gather(bf16[1,1,16]{2,1,0:T(2,128)(2,1)S(1)} %get-tuple-element.50), channel_id=1, replica_groups=mesh['sp_0'=8,'sp_1'=8,'fs'=4,'tp'=2] {'sp_0'}, dimensions={0}, use_global_device_ids=true | all-gather | bytes 288 | tf_op jit(solution)/shard_map/all_gather | solution.py:71
  272.3 4.7 %collective-permute-start.2 = (bf16[256,512]{1,0:T(8,128)(2,1)S(1)}, bf16[256,512]{1,0:T(8,128)(2,1)}, u32[]{:S(2)}, u32[]{:S(2)}) collective-permute-start(bf16[256,512]{1,0:T(8,128)(2,1)S(1)} %slice.520), channel_id=1, source_target_pairs={{0,8},{8,16},{16,24},{24,32},{32,40},{40,48},{48,56},{56,64},{64,7... | collective-permute-start | bytes 786440 | tf_op jit(solution)/shard_map/ppermute | solution.py:24
  279.6 2.5 maximum_convert_fusion.1
  282.0 2.3 reshape.1139
  287.9 1.9 slice_convert_fusion.15
  290.6 1.9 slice_convert_fusion.7
  292.7 1.8 fusion.242
  299.5 1.8 copy.77
  301.4 2.1 reshape.1087
  303.7 1.8 fusion.241
  310.6 1.8 copy.94
  312.4 3.0 reshape.1094
  315.5 2.3 rev.19
  317.7 1.6 multiply_reduce_fusion
  319.7 31.8 %all-gather.21.cloned.1.call-done = bf16[1536,1024]{1,0:T(8,128)(2,1)} async-done(((bf16[1536,256]{1,0:T(8,128)(2,1)}), bf16[1536,1024]{1,0:T(8,128)(2,1)}) %all-gather.21.cloned.1.call-update) | async-done | bytes 3145744 | tf_op jit(solution)/shard_map/all_gather | solution.py:38
  351.5 2.4 fusion.1
  353.9 1.8 fusion.35
  355.7 5.8 %all_to_all.10 = bf16[2,128,1024]{2,1,0:T(8,128)(2,1)S(1)} all-to-all(bf16[2,128,1024]{2,1,0:T(8,128)(2,1)S(1)} %bitcast.452), channel_id=1, replica_groups=mesh['sp_0'=8,'sp_1'=8,'fs'=4,'tp'=2] {'tp'}, dimensions={0} | all-to-all | bytes 1048576 | tf_op jit(solution)/shard_map/all_to_all | solution.py:93
  (373 shorter events, 73.8 us)
Async XLA Ops:
  6.5 280.2 %copy-start = (bf16[4,256,256]{2,1,0:T(8,128)(2,1)S(1)}, bf16[4,256,256]{2,1,0:T(8,128)(2,1)}, u32[]{:S(2)}) copy-start(bf16[4,256,256]{2,1,0:T(8,128)(2,1)} %param.28) | copy-start | bytes 1572868
  6.5 16.7 %copy-start.95 = (f32[2,32]{1,0:T(2,128)S(1)}, f32[2,32]{1,0:T(2,128)}, u32[]{:S(2)}) copy-start(f32[2,32]{1,0:T(2,128)} %param.25) | copy-start | bytes 772
  6.5 16.7 %copy-start.47 = (bf16[1024,2,32]{0,2,1:T(8,128)(2,1)S(1)}, bf16[1024,2,32]{0,2,1:T(8,128)(2,1)}, u32[]{:S(2)}) copy-start(bf16[1024,2,32]{0,2,1:T(8,128)(2,1)} %param.22) | copy-start | bytes 393220
  6.5 99.4 %all-gather.11.cloned.1.call-start = ((), (), s32[]{:S(2)}) async-start(), calls=%async_computation.2 | async-start | bytes 6389760 | tf_op jit(solution)/shard_map/all_gather | solution.py:226
  10.3 14.5 %copy-start.48 = (f32[1,256,2,16]{1,3,2,0:T(8,128)S(1)}, f32[1,256,2,16]{1,3,2,0:T(8,128)}, u32[]{:S(2)}) copy-start(f32[1,256,2,16]{1,3,2,0:T(8,128)} %param.26) | copy-start | bytes 98308
  12.0 14.8 %copy-start.41 = (bf16[5,2,512]{2,1,0:T(2,128)(2,1)S(1)}, bf16[5,2,512]{2,1,0:T(2,128)(2,1)}, u32[]{:S(2)}) copy-start(bf16[5,2,512]{2,1,0:T(2,128)(2,1)} %param.24) | copy-start | bytes 30724
  12.0 15.1 %copy-start.57 = (bf16[5,2048]{1,0:T(8,128)(2,1)S(1)}, bf16[5,2048]{1,0:T(8,128)(2,1)}, u32[]{:S(2)}) copy-start(bf16[5,2048]{1,0:T(8,128)(2,1)} %param.23) | copy-start | bytes 61444
  12.9 11.7 %all-to-all-start = ((bf16[2,256,512]{1,2,0:T(8,128)(2,1)}), bf16[2,256,512]{1,2,0:T(8,128)(2,1)S(1)}, u32[]{:S(2)}, u32[]{:S(2)}) async-start(bf16[2,256,512]{1,2,0:T(8,128)(2,1)} %broadcast_in_dim.44), calls=%async_computation | async-start | bytes 1048576 | tf_op jit(solution)/shard_map/all_to_all | solution.py:43
  23.2 141.3 %all-gather.13.cloned.1.call-start = ((), (), s32[]{:S(2)}) async-start(), calls=%async_computation.3 | async-start | bytes 2359296 | tf_op jit(solution)/shard_map/all_gather | solution.py:71
  26.2 84.4 %copy-start.43 = (f32[2,2,8]{2,1,0:T(2,128)}, f32[2,2,8]{2,1,0:T(2,128)S(1)}, u32[]{:S(2)}) copy-start(f32[2,2,8]{2,1,0:T(2,128)S(1)} %slice_reduce_fusion.1) | copy-start | bytes 388
  26.9 103.5 %copy-start.37 = (f32[2,2,8]{2,1,0:T(2,128)}, f32[2,2,8]{2,1,0:T(2,128)S(1)}, u32[]{:S(2)}) copy-start(f32[2,2,8]{2,1,0:T(2,128)S(1)} %fusion.249) | copy-start | bytes 388
  110.5 6.3 %copy-start.19 = (bf16[256,3072]{1,0:T(8,128)(2,1)}, bf16[256,3072]{1,0:T(8,128)(2,1)S(1)}, u32[]{:S(2)}) copy-start(bf16[256,3072]{1,0:T(8,128)(2,1)S(1)} %fusion) | copy-start | bytes 4718596
  110.6 5.5 %collective-permute-start.1 = (bf16[2,1536]{1,0:T(2,128)(2,1)S(1)}, bf16[2,1536]{1,0:T(2,128)(2,1)S(1)}, u32[]{:S(2)}, u32[]{:S(2)}) collective-permute-start(bf16[2,1536]{1,0:T(2,128)(2,1)S(1)} %get-tuple-element.95), channel_id=1, source_target_pairs={{8,0},{16,8},{24,16},{32,24},{40,32},{48,40},{56,48},{64,56},{72,6... | collective-permute-start | bytes 18440 | tf_op jit(solution)/shard_map/ppermute | solution.py:27
  111.9 4.8 %collective-permute-start = (bf16[2,1536]{1,0:T(2,128)(2,1)S(1)}, bf16[2,1536]{1,0:T(2,128)(2,1)S(1)}, u32[]{:S(2)}, u32[]{:S(2)}) collective-permute-start(bf16[2,1536]{1,0:T(2,128)(2,1)S(1)} %get-tuple-element.94), channel_id=1, source_target_pairs={{0,8},{8,16},{16,24},{24,32},{32,40},{40,48},{48,56},{56,64},{64,7... | collective-permute-start | bytes 18440 | tf_op jit(solution)/shard_map/ppermute | solution.py:24
  120.9 3.7 copy-start.24
  122.3 86.4 %all-gather.17.cloned.1.call-start = ((), (), s32[]{:S(2)}) async-start(), calls=%async_computation.5 | async-start | bytes 2359296 | tf_op jit(solution)/shard_map/all_gather | solution.py:71
  128.9 38.3 %copy-start.22 = (bf16[2,2,8,64,128]{4,3,2,1,0:T(8,128)(2,1)}, bf16[2,2,8,64,128]{4,3,2,1,0:T(8,128)(2,1)S(1)}, u32[]{:S(2)}) copy-start(bf16[2,2,8,64,128]{4,3,2,1,0:T(8,128)(2,1)S(1)} %fusion.43) | copy-start | bytes 1572868
  130.3 36.9 %copy-start.40 = (f32[2,2,8]{2,1,0:T(2,128)S(1)}, f32[2,2,8]{2,1,0:T(2,128)}, u32[]{:S(2)}) copy-start(f32[2,2,8]{2,1,0:T(2,128)} %copy-done.39) | copy-start | bytes 388
  130.4 162.1 %all-gather.15.cloned.1.call-start = ((), (), s32[]{:S(2)}) async-start(), calls=%async_computation.4 | async-start | bytes 2359296 | tf_op jit(solution)/shard_map/all_gather | solution.py:71
  167.2 44.4 %copy-start.20 = (bf16[1024,256]{1,0:T(8,128)(2,1)S(1)}, bf16[1024,256]{1,0:T(8,128)(2,1)}, u32[]{:S(2)}) copy-start(bf16[1024,256]{1,0:T(8,128)(2,1)} %param.30) | copy-start | bytes 1572868
  167.2 44.5 %copy-start.29 = (bf16[512,256]{1,0:T(8,128)(2,1)S(1)}, bf16[512,256]{1,0:T(8,128)(2,1)}, u32[]{:S(2)}) copy-start(bf16[512,256]{1,0:T(8,128)(2,1)} %param.31) | copy-start | bytes 786436
  167.2 136.4 %all-gather.19.cloned.1.call-start = ((), (), s32[]{:S(2)}) async-start(), calls=%async_computation.6 | async-start | bytes 2359296 | tf_op jit(solution)/shard_map/all_gather | solution.py:71
  211.5 3.1 copy-start.46
  211.5 3.8 %dynamic-slice-start = ((f32[2048]{0:T(1024)}, s32[]{:T(128)}), f32[1024]{0:T(1024)S(1)}, s32[]{:S(2)}) async-start(f32[2048]{0:T(1024)} %param.27, s32[]{:T(128)} %select_n.565), calls=%async_computation.8 | async-start | bytes 8704 | tf_op jit(solution)/shard_map/dynamic_slice | solution.py:283
  211.5 55.1 %copy-start.94 = (f32[1024]{0:T(1024)S(1)}, f32[1024]{0:T(1024)}, u32[]{:S(2)}) copy-start(f32[1024]{0:T(1024)} %param.29) | copy-start | bytes 12292
  211.6 139.9 %all-gather.21.cloned.1.call-start = ((), (), s32[]{:S(2)}) async-start(), calls=%async_computation.7 | async-start | bytes 3932160 | tf_op jit(solution)/shard_map/all_gather | solution.py:38
  271.0 8.4 %collective-permute-start.3 = (bf16[256,512]{1,0:T(8,128)(2,1)S(1)}, bf16[256,512]{1,0:T(8,128)(2,1)}, u32[]{:S(2)}, u32[]{:S(2)}) collective-permute-start(bf16[256,512]{1,0:T(8,128)(2,1)S(1)} %slice.520), channel_id=1, source_target_pairs={{8,0},{16,8},{24,16},{32,24},{40,32},{48,40},{56,48},{64,56},{72,6... | collective-permute-start | bytes 786440 | tf_op jit(solution)/shard_map/ppermute | solution.py:27
  272.3 7.3 %collective-permute-start.2 = (bf16[256,512]{1,0:T(8,128)(2,1)S(1)}, bf16[256,512]{1,0:T(8,128)(2,1)}, u32[]{:S(2)}, u32[]{:S(2)}) collective-permute-start(bf16[256,512]{1,0:T(8,128)(2,1)S(1)} %slice.520), channel_id=1, source_target_pairs={{0,8},{8,16},{16,24},{24,32},{32,40},{40,48},{48,56},{56,64},{64,7... | collective-permute-start | bytes 786440 | tf_op jit(solution)/shard_map/ppermute | solution.py:24
  287.9 2.7 copy-start.4
  292.6 2.5 copy-start.18
  292.6 2.5 copy-start.77
  353.9 8.4 %copy-start.1 = (bf16[4,256,256]{2,1,0:T(8,128)(2,1)S(1)}, bf16[4,256,256]{2,1,0:T(8,128)(2,1)}, u32[]{:S(2)}) copy-start(bf16[4,256,256]{2,1,0:T(8,128)(2,1)} %param.28) | copy-start | bytes 1572868
  (78 other events, 143.3 us)
Sparse Core Ops, SparseCore 0:
  11.0 94.8 all-gather.10
  122.5 41.9 all-gather.12
  166.5 42.1 all-gather.16
  210.7 42.7 all-gather.14
  255.5 47.0 all-gather.18
  304.5 46.9 all-gather.20
where the time goes:
time: 370 us; the launch traced here: 369 us
  waiting for transfers between devices  163 us (44%)
  local copies, waits for them, and re-layouts  62.2 us (17%)
  blocking collectives  57.1 us (15%)
  other arithmetic  32.1 us (9%)
  starting transfers between devices  21.7 us (6%)
  matrix products  18.1 us (5%)
  between operations  15.2 us (4%)
    all_gather x1, waiting for transfers between devices, body(): lax.all_gather(stacked, SP, axis=0, tiled=True)  78.8 us
    all_gather x4, blocking collectives, prefix_by_axis(): lax.all_gather(part.astype(kind), axis)  51.3 us
    all_gather x4, waiting for transfers between devices, prefix_by_axis(): lax.all_gather(part.astype(kind), axis)  49.8 us
    all_gather x1, waiting for transfers between devices, sent_together(): lax.all_gather(both, axis, axis=dim, tiled=True)  31.8 us
    exp x30, local copies, waits for them, and re-layouts, merge_states(): jnp.exp(later[0])[:, None, None]  19.4 us
    all_to_all x1, starting transfers between devices, sent_to_all(): lax.all_to_all(jnp.broadcast_to(value[None], (devices, *value.shape)), ax...  10.3 us
    ppermute x2, starting transfers between devices, with_halo(): lax.ppermute(lax.slice_in_dim(block, block.shape[dim] - width, None, axis...  8.68 us
    unnamed x205, local copies, waits for them, and re-layouts  7.85 us
  transfers between devices with their start and end apart: 11, of which 7 were waited for; matrix products, arithmetic and copies ran while one was open for 24% of the time, Pallas kernels for 0%

commit v1 on v0

--- a/solution.py
+++ b/solution.py
@@ -223,7 +223,7 @@
     stacked = jnp.concatenate([w_inner, w_write, w_read, w_gate, w_pool_in], axis=1)
     projected = jnp.dot(
         whole_rows,
-        lax.all_gather(stacked, SP, axis=0, tiled=True),
+        jnp.concatenate(lax.all_to_all(jnp.stack([stacked] * lax.axis_size(SP)), SP, 0, 0), axis=0),
         preferred_element_type=jnp.float32,
     )
     projected = projected.astype(jnp.bfloat16)

time: 370 us -> 519 us (1.40)
  waiting for transfers between devices: 163 us -> 253 us
  blocking collectives: 57.1 us -> 92.8 us
  starting transfers between devices: 21.7 us -> 45.7 us
    all_to_all x0 -> x1, waiting for transfers between devices: none -> 172 us  [body(): lax.all_to_all(jnp.stack([stacked] * lax.axis_size(SP)), SP, 0, 0)]
    all_gather x1 -> x0, waiting for transfers between devices: 78.8 us -> none  [body(): lax.all_gather(stacked, SP, axis=0, tiled=True)]
    all_gather x4, blocking collectives: 51.3 us -> 87 us  [prefix_by_axis(): lax.all_gather(part.astype(kind), axis)]
    ppermute x2, starting transfers between devices: 8.68 us -> 21.3 us  [with_halo(): lax.ppermute(lax.slice_in_dim(block, block.shape[dim] - width, None, axis...]
    all_to_all x0 -> x1, starting transfers between devices: none -> 11.3 us  [body(): lax.all_to_all(jnp.stack([stacked] * lax.axis_size(SP)), SP, 0, 0)]
  transfers between devices with their start and end apart: 11 -> 11, of which waited for: 7 -> 7; matrix products, arithmetic and copies ran while one was open for 24% -> 17% of each run, Pallas kernels for 0% -> 0%
where the time goes in v1:
time: 519 us; the launch traced here: 518 us
  waiting for transfers between devices  253 us (49%)
  blocking collectives  92.8 us (18%)
  local copies, waits for them, and re-layouts  61.4 us (12%)
  starting transfers between devices  45.7 us (9%)
  other arithmetic  32.1 us (6%)
  matrix products  18.1 us (3%)
  between operations  15 us (3%)
    all_to_all x1, waiting for transfers between devices, body(): lax.all_to_all(jnp.stack([stacked] * lax.axis_size(SP)), SP, 0, 0)  172 us
    all_gather x4, blocking collectives, prefix_by_axis(): lax.all_gather(part.astype(kind), axis)  87 us
    all_gather x4, waiting for transfers between devices, prefix_by_axis(): lax.all_gather(part.astype(kind), axis)  47.9 us
    all_gather x1, waiting for transfers between devices, sent_together(): lax.all_gather(both, axis, axis=dim, tiled=True)  31.4 us
    ppermute x2, starting transfers between devices, with_halo(): lax.ppermute(lax.slice_in_dim(block, block.shape[dim] - width, None, axis...  21.3 us
    exp x30, local copies, waits for them, and re-layouts, merge_states(): jnp.exp(later[0])[:, None, None]  19.4 us
    all_to_all x1, starting transfers between devices, body(): lax.all_to_all(jnp.stack([stacked] * lax.axis_size(SP)), SP, 0, 0)  11.3 us
  transfers between devices with their start and end apart: 11, of which 7 were waited for; matrix products, arithmetic and copies ran while one was open for 17% of the time, Pallas kernels for 0%

profile of v1, /device:TPU:1, one launch (start us, length us, event | category | flops | bytes accessed | tf_op | source)
XLA Modules:
  0.0 518.3 jit_solution(5871400976904105801)
XLA Ops:
  8.5 10.3 %all-to-all-start.1 = ((bf16[2,256,512]{1,2,0:T(8,128)(2,1)}), bf16[2,256,512]{1,2,0:T(8,128)(2,1)S(1)}, u32[]{:S(2)}, u32[]{:S(2)}) async-start(bf16[2,256,512]{1,2,0:T(8,128)(2,1)} %broadcast_in_dim.44), calls=%async_computation.1 | async-start | bytes 1048576 | tf_op jit(solution)/shard_map/all_to_all | solution.py:43
  20.2 3.4 stack.2
  23.7 11.3 %all-to-all-start = ((bf16[64,16,3072]{2,1,0:T(8,128)(2,1)}), bf16[64,16,3072]{2,1,0:T(8,128)(2,1)}, u32[]{:S(2)}, u32[]{:S(2)}) async-start(bf16[64,16,3072]{2,1,0:T(8,128)(2,1)} %stack.2), calls=%async_computation | async-start | bytes 12582912 | tf_op jit(solution)/shard_map/all_to_all | solution.py:226
  37.7 171.7 %all-to-all-done = bf16[64,16,3072]{2,1,0:T(8,128)(2,1)} async-done(((bf16[64,16,3072]{2,1,0:T(8,128)(2,1)}), bf16[64,16,3072]{2,1,0:T(8,128)(2,1)}, u32[]{:S(2)}, u32[]{:S(2)}) %all-to-all-start) | async-done | bytes 6291488 | tf_op jit(solution)/shard_map/all_to_all | solution.py:226
  209.4 4.6 fusion
  215.4 16.6 %collective-permute-start = (bf16[2,1536]{1,0:T(2,128)(2,1)S(1)}, bf16[2,1536]{1,0:T(2,128)(2,1)S(1)}, u32[]{:S(2)}, u32[]{:S(2)}) collective-permute-start(bf16[2,1536]{1,0:T(2,128)(2,1)S(1)} %get-tuple-element.94), channel_id=1, source_target_pairs={{0,8},{8,16},{16,24},{24,32},{32,40},{40,48},{48,56},{56,64},{64,7... | collective-permute-start | bytes 18440 | tf_op jit(solution)/shard_map/ppermute | solution.py:24
  242.2 1.7 reshape.1095
  246.6 49.5 %all-gather = bf16[8,1,16]{2,1,0:T(2,128)(2,1)S(1)} all-gather(bf16[1,1,16]{2,1,0:T(2,128)(2,1)S(1)} %reshape.1184), channel_id=1, replica_groups=mesh['sp_0'=8,'sp_1'=8,'fs'=4,'tp'=2] {'sp_1'}, dimensions={0}, use_global_device_ids=true | all-gather | bytes 288 | tf_op jit(solution)/shard_map/all_gather | solution.py:71
  296.2 18.0 %all-gather.10.cloned.1.call-done = bf16[8,16,64,128]{3,2,1,0:T(8,128)(2,1)} async-done(((bf16[1,16,64,128]{3,2,1,0:T(8,128)(2,1)}), bf16[8,16,64,128]{3,2,1,0:T(8,128)(2,1)}) %all-gather.10.cloned.1.call-update) | async-done | bytes 2097168 | tf_op jit(solution)/shard_map/all_gather | solution.py:71
  314.2 2.7 add_convert_fusion.1
  317.2 11.3 %all-gather.2 = bf16[8,1,16]{2,1,0:T(2,128)(2,1)S(1)} all-gather(bf16[1,1,16]{2,1,0:T(2,128)(2,1)S(1)} %reshape.1188), channel_id=1, replica_groups=mesh['sp_0'=8,'sp_1'=8,'fs'=4,'tp'=2] {'sp_1'}, dimensions={0}, use_global_device_ids=true | all-gather | bytes 288 | tf_op jit(solution)/shard_map/all_gather | solution.py:71
  328.6 29.9 %all-gather.14.cloned.1.call-done = bf16[8,16,64,128]{3,2,1,0:T(8,128)(2,1)} async-done(((bf16[1,16,64,128]{3,2,1,0:T(8,128)(2,1)}), bf16[8,16,64,128]{3,2,1,0:T(8,128)(2,1)}) %all-gather.14.cloned.1.call-update) | async-done | bytes 2097168 | tf_op jit(solution)/shard_map/all_gather | solution.py:71
  358.5 2.7 add_convert_fusion
  371.4 13.8 %all-gather.3 = bf16[8,1,16]{2,1,0:T(2,128)(2,1)S(1)} all-gather(bf16[1,1,16]{2,1,0:T(2,128)(2,1)S(1)} %get-tuple-element.46), channel_id=1, replica_groups=mesh['sp_0'=8,'sp_1'=8,'fs'=4,'tp'=2] {'sp_0'}, dimensions={0}, use_global_device_ids=true | all-gather | bytes 288 | tf_op jit(solution)/shard_map/all_gather | solution.py:71
  385.2 12.3 %all-gather.1 = bf16[8,1,16]{2,1,0:T(2,128)(2,1)S(1)} all-gather(bf16[1,1,16]{2,1,0:T(2,128)(2,1)S(1)} %get-tuple-element.50), channel_id=1, replica_groups=mesh['sp_0'=8,'sp_1'=8,'fs'=4,'tp'=2] {'sp_0'}, dimensions={0}, use_global_device_ids=true | all-gather | bytes 288 | tf_op jit(solution)/shard_map/all_gather | solution.py:71
  422.1 4.7 collective-permute-start.2
  429.4 2.5 maximum_convert_fusion.1
  431.8 2.3 reshape.1145
  437.7 1.9 slice_convert_fusion.15
  440.4 1.9 slice_convert_fusion.7
  442.5 1.8 fusion.242
  449.4 1.8 copy.77
  451.2 2.1 reshape.1093
  453.5 1.8 fusion.241
  460.4 1.8 copy.94
  462.2 3.0 reshape.1100
  465.3 2.3 rev.19
  467.5 1.7 multiply_reduce_fusion
  469.6 31.4 %all-gather.18.cloned.1.call-done = bf16[1536,1024]{1,0:T(8,128)(2,1)} async-done(((bf16[1536,256]{1,0:T(8,128)(2,1)}), bf16[1536,1024]{1,0:T(8,128)(2,1)}) %all-gather.18.cloned.1.call-update) | async-done | bytes 3145744 | tf_op jit(solution)/shard_map/all_gather | solution.py:38
  501.0 2.4 fusion.1
  503.3 1.8 fusion.35
  505.1 5.8 %all_to_all.15 = bf16[2,128,1024]{2,1,0:T(8,128)(2,1)S(1)} all-to-all(bf16[2,128,1024]{2,1,0:T(8,128)(2,1)S(1)} %bitcast.453), channel_id=1, replica_groups=mesh['sp_0'=8,'sp_1'=8,'fs'=4,'tp'=2] {'tp'}, dimensions={0} | all-to-all | bytes 1048576 | tf_op jit(solution)/shard_map/all_to_all | solution.py:93
  (381 shorter events, 72.3 us)
Async XLA Ops:
  6.5 430.0 %copy-start = (bf16[4,256,256]{2,1,0:T(8,128)(2,1)S(1)}, bf16[4,256,256]{2,1,0:T(8,128)(2,1)}, u32[]{:S(2)}) copy-start(bf16[4,256,256]{2,1,0:T(8,128)(2,1)} %param.28) | copy-start | bytes 1572868
  6.5 12.3 %copy-start.47 = (bf16[16,1024]{1,0:T(8,128)(2,1)S(1)}, bf16[16,1024]{1,0:T(8,128)(2,1)}, u32[]{:S(2)}) copy-start(bf16[16,1024]{1,0:T(8,128)(2,1)} %param.17) | copy-start | bytes 98308
  6.5 12.3 %copy-start.60 = (bf16[16,256]{1,0:T(8,128)(2,1)S(1)}, bf16[16,256]{1,0:T(8,128)(2,1)}, u32[]{:S(2)}) copy-start(bf16[16,256]{1,0:T(8,128)(2,1)} %param.19) | copy-start | bytes 24580
  6.5 12.3 %copy-start.61 = (bf16[16,256]{1,0:T(8,128)(2,1)S(1)}, bf16[16,256]{1,0:T(8,128)(2,1)}, u32[]{:S(2)}) copy-start(bf16[16,256]{1,0:T(8,128)(2,1)} %param.20) | copy-start | bytes 24580
  6.5 12.3 %copy-start.48 = (bf16[16,1024]{1,0:T(8,128)(2,1)S(1)}, bf16[16,1024]{1,0:T(8,128)(2,1)}, u32[]{:S(2)}) copy-start(bf16[16,1024]{1,0:T(8,128)(2,1)} %param.18) | copy-start | bytes 98308
  6.5 12.4 %copy-start.50 = (bf16[16,512]{1,0:T(8,128)(2,1)S(1)}, bf16[16,512]{1,0:T(8,128)(2,1)}, u32[]{:S(2)}) copy-start(bf16[16,512]{1,0:T(8,128)(2,1)} %param.21) | copy-start | bytes 49156
  8.5 11.7 %all-to-all-start.1 = ((bf16[2,256,512]{1,2,0:T(8,128)(2,1)}), bf16[2,256,512]{1,2,0:T(8,128)(2,1)S(1)}, u32[]{:S(2)}, u32[]{:S(2)}) async-start(bf16[2,256,512]{1,2,0:T(8,128)(2,1)} %broadcast_in_dim.44), calls=%async_computation.1 | async-start | bytes 1048576 | tf_op jit(solution)/shard_map/all_to_all | solution.py:43
  23.6 11.4 %copy-start.99 = (f32[2,32]{1,0:T(2,128)S(1)}, f32[2,32]{1,0:T(2,128)}, u32[]{:S(2)}) copy-start(f32[2,32]{1,0:T(2,128)} %param.25) | copy-start | bytes 772
  23.6 11.5 %copy-start.46 = (bf16[1024,2,32]{0,2,1:T(8,128)(2,1)S(1)}, bf16[1024,2,32]{0,2,1:T(8,128)(2,1)}, u32[]{:S(2)}) copy-start(bf16[1024,2,32]{0,2,1:T(8,128)(2,1)} %param.22) | copy-start | bytes 393220
  23.6 11.7 %copy-start.49 = (f32[1,256,2,16]{1,3,2,0:T(8,128)S(1)}, f32[1,256,2,16]{1,3,2,0:T(8,128)}, u32[]{:S(2)}) copy-start(f32[1,256,2,16]{1,3,2,0:T(8,128)} %param.26) | copy-start | bytes 98308
  23.6 13.8 %copy-start.40 = (bf16[5,2,512]{2,1,0:T(2,128)(2,1)S(1)}, bf16[5,2,512]{2,1,0:T(2,128)(2,1)}, u32[]{:S(2)}) copy-start(bf16[5,2,512]{2,1,0:T(2,128)(2,1)} %param.24) | copy-start | bytes 30724
  23.6 14.0 %copy-start.59 = (bf16[5,2048]{1,0:T(8,128)(2,1)S(1)}, bf16[5,2048]{1,0:T(8,128)(2,1)}, u32[]{:S(2)}) copy-start(bf16[5,2048]{1,0:T(8,128)(2,1)} %param.23) | copy-start | bytes 61444
  23.7 185.7 %all-to-all-start = ((bf16[64,16,3072]{2,1,0:T(8,128)(2,1)}), bf16[64,16,3072]{2,1,0:T(8,128)(2,1)}, u32[]{:S(2)}, u32[]{:S(2)}) async-start(bf16[64,16,3072]{2,1,0:T(8,128)(2,1)} %stack.2), calls=%async_computation | async-start | bytes 12582912 | tf_op jit(solution)/shard_map/all_to_all | solution.py:226
  35.0 279.2 %all-gather.10.cloned.1.call-start = ((), (), s32[]{:S(2)}) async-start(), calls=%async_computation.3 | async-start | bytes 2359296 | tf_op jit(solution)/shard_map/all_gather | solution.py:71
  36.8 177.3 %copy-start.42 = (f32[2,2,8]{2,1,0:T(2,128)}, f32[2,2,8]{2,1,0:T(2,128)S(1)}, u32[]{:S(2)}) copy-start(f32[2,2,8]{2,1,0:T(2,128)S(1)} %slice_reduce_fusion.1) | copy-start | bytes 388
  37.5 208.9 %copy-start.36 = (f32[2,2,8]{2,1,0:T(2,128)}, f32[2,2,8]{2,1,0:T(2,128)S(1)}, u32[]{:S(2)}) copy-start(f32[2,2,8]{2,1,0:T(2,128)S(1)} %fusion.249) | copy-start | bytes 388
  214.0 18.9 %copy-start.19 = (bf16[256,3072]{1,0:T(8,128)(2,1)}, bf16[256,3072]{1,0:T(8,128)(2,1)S(1)}, u32[]{:S(2)}) copy-start(bf16[256,3072]{1,0:T(8,128)(2,1)S(1)} %fusion) | copy-start | bytes 4718596
  214.1 18.0 %collective-permute-start.1 = (bf16[2,1536]{1,0:T(2,128)(2,1)S(1)}, bf16[2,1536]{1,0:T(2,128)(2,1)S(1)}, u32[]{:S(2)}, u32[]{:S(2)}) collective-permute-start(bf16[2,1536]{1,0:T(2,128)(2,1)S(1)} %get-tuple-element.95), channel_id=1, source_target_pairs={{8,0},{16,8},{24,16},{32,24},{40,32},{48,40},{56,48},{64,56},{72,6... | collective-permute-start | bytes 18440 | tf_op jit(solution)/shard_map/ppermute | solution.py:27
  215.4 17.3 %collective-permute-start = (bf16[2,1536]{1,0:T(2,128)(2,1)S(1)}, bf16[2,1536]{1,0:T(2,128)(2,1)S(1)}, u32[]{:S(2)}, u32[]{:S(2)}) collective-permute-start(bf16[2,1536]{1,0:T(2,128)(2,1)S(1)} %get-tuple-element.94), channel_id=1, source_target_pairs={{0,8},{8,16},{16,24},{24,32},{32,40},{40,48},{48,56},{56,64},{64,7... | collective-permute-start | bytes 18440 | tf_op jit(solution)/shard_map/ppermute | solution.py:24
  238.4 120.1 %all-gather.14.cloned.1.call-start = ((), (), s32[]{:S(2)}) async-start(), calls=%async_computation.5 | async-start | bytes 2359296 | tf_op jit(solution)/shard_map/all_gather | solution.py:71
  245.0 72.0 %copy-start.22 = (bf16[2,2,8,64,128]{4,3,2,1,0:T(8,128)(2,1)}, bf16[2,2,8,64,128]{4,3,2,1,0:T(8,128)(2,1)S(1)}, u32[]{:S(2)}) copy-start(bf16[2,2,8,64,128]{4,3,2,1,0:T(8,128)(2,1)S(1)} %fusion.43) | copy-start | bytes 1572868
  246.4 70.6 %copy-start.39 = (f32[2,2,8]{2,1,0:T(2,128)S(1)}, f32[2,2,8]{2,1,0:T(2,128)}, u32[]{:S(2)}) copy-start(f32[2,2,8]{2,1,0:T(2,128)} %copy-done.38) | copy-start | bytes 388
  246.4 195.9 %all-gather.12.cloned.1.call-start = ((), (), s32[]{:S(2)}) async-start(), calls=%async_computation.4 | async-start | bytes 2359296 | tf_op jit(solution)/shard_map/all_gather | solution.py:71
  316.9 44.4 %copy-start.20 = (bf16[1024,256]{1,0:T(8,128)(2,1)S(1)}, bf16[1024,256]{1,0:T(8,128)(2,1)}, u32[]{:S(2)}) copy-start(bf16[1024,256]{1,0:T(8,128)(2,1)} %param.30) | copy-start | bytes 1572868
  316.9 44.4 %copy-start.29 = (bf16[512,256]{1,0:T(8,128)(2,1)S(1)}, bf16[512,256]{1,0:T(8,128)(2,1)}, u32[]{:S(2)}) copy-start(bf16[512,256]{1,0:T(8,128)(2,1)} %param.31) | copy-start | bytes 786436
  317.0 136.5 %all-gather.16.cloned.1.call-start = ((), (), s32[]{:S(2)}) async-start(), calls=%async_computation.6 | async-start | bytes 2359296 | tf_op jit(solution)/shard_map/all_gather | solution.py:71
  361.2 3.7 dynamic-slice-start
  361.2 55.2 %copy-start.98 = (f32[1024]{0:T(1024)S(1)}, f32[1024]{0:T(1024)}, u32[]{:S(2)}) copy-start(f32[1024]{0:T(1024)} %param.29) | copy-start | bytes 12292
  361.3 139.7 %all-gather.18.cloned.1.call-start = ((), (), s32[]{:S(2)}) async-start(), calls=%async_computation.7 | async-start | bytes 3932160 | tf_op jit(solution)/shard_map/all_gather | solution.py:38
  420.8 8.4 %collective-permute-start.3 = (bf16[256,512]{1,0:T(8,128)(2,1)S(1)}, bf16[256,512]{1,0:T(8,128)(2,1)}, u32[]{:S(2)}, u32[]{:S(2)}) collective-permute-start(bf16[256,512]{1,0:T(8,128)(2,1)S(1)} %slice.520), channel_id=1, source_target_pairs={{8,0},{16,8},{24,16},{32,24},{40,32},{48,40},{56,48},{64,56},{72,6... | collective-permute-start | bytes 786440 | tf_op jit(solution)/shard_map/ppermute | solution.py:27
  422.1 7.3 %collective-permute-start.2 = (bf16[256,512]{1,0:T(8,128)(2,1)S(1)}, bf16[256,512]{1,0:T(8,128)(2,1)}, u32[]{:S(2)}, u32[]{:S(2)}) collective-permute-start(bf16[256,512]{1,0:T(8,128)(2,1)S(1)} %slice.520), channel_id=1, source_target_pairs={{0,8},{8,16},{16,24},{24,32},{32,40},{40,48},{48,56},{56,64},{64,7... | collective-permute-start | bytes 786440 | tf_op jit(solution)/shard_map/ppermute | solution.py:24
  503.3 8.4 %copy-start.1 = (bf16[4,256,256]{2,1,0:T(8,128)(2,1)S(1)}, bf16[4,256,256]{2,1,0:T(8,128)(2,1)}, u32[]{:S(2)}) copy-start(bf16[4,256,256]{2,1,0:T(8,128)(2,1)} %param.28) | copy-start | bytes 1572868
  (82 other events, 157.6 us)
Sparse Core Ops, SparseCore 0:
  238.5 75.6 all-gather.9
  316.3 42.1 all-gather.13
  360.6 42.7 all-gather.11
  405.3 46.8 all-gather.15
  454.1 46.7 all-gather.17
